TPU v7x, 32 devices: a whole 2x2x4 slice. The times are simulated.
32 devices in a mesh: sp: 8 (over z, y), tp: 4 (over x, core).
Axes of the slice: x: 2, y: 2, z: 4, core: 2. Of those that a mesh axis runs over, the one named last changes fastest.
Arguments:
- tokens: bfloat16 [4, 512, 1024], P(None, 'sp', 'tp'), may hold values from -6 to 6
- norm_gain: float32 [4, 1024], replicated, may hold values from 0.1 to 1.9
- val_weight: bfloat16 [4, 1024, 512], P(None, 'sp', 'tp'), may hold values from -0.1875 to 0.1875
- gate_weight: bfloat16 [4, 1024, 512], P(None, 'sp', 'tp'), may hold values from -0.1875 to 0.1875
- conv_taps: float32 [4, 31, 512], P(None, None, 'tp'), may hold values from -1 to 1
- conv_bias: float32 [4, 512], P(None, 'tp'), may hold values from -3 to 3
- ln_gain: float32 [4, 512], P(None, 'tp'), may hold values from 0.1 to 1.9
- ln_shift: float32 [4, 512], P(None, 'tp'), may hold values from -3 to 3
- out_weight: bfloat16 [4, 512, 1024], P(None, 'tp', 'sp'), may hold values from -0.25 to 0.25
Outputs:
- stream: bfloat16 [4, 512, 1024], P(None, 'sp', 'tp')
All inputs are finite; a program needn't handle non-finite values.
Results may differ from a plain program's by a relative error of at most 0.02.
Values may be sent and summed in bfloat16 or wider, within the bound.
A program may use at most 64 MiB of HBM per device.

v0:
```python
from functools import partial

import jax
import jax.numpy as jnp
from jax import lax
from jax.sharding import PartitionSpec as P

LAYERS = 4


epsilon = 1e-06


def over_all(shard, axis, dim, absorb, state):
    everything = jax.tree.map(lambda a: lax.all_gather(a, axis, axis=dim, tiled=True), shard)
    return absorb(state, everything, jnp.int32(0))


def with_halo(shard, sides, width, wrap):
    for axis, dim in sides:
        size, length = lax.axis_size(axis), shard.shape[dim]
        up = [(i, (i + 1) % size) for i in range(size if wrap else size - 1)]
        down = [(j, i) for i, j in up]
        last = lax.slice_in_dim(shard, length - width, length, axis=dim)
        initial = lax.slice_in_dim(shard, 0, width, axis=dim)
        before = lax.ppermute(last, axis, up)
        after = lax.ppermute(initial, axis, down)
        shard = jnp.concatenate([before, shard, after], axis=dim)
    return shard


def over_all_2(shard, axis, dim, work):
    return work(lax.all_gather(shard, axis, axis=dim, tiled=True), jnp.int32(0))


def depthwise(padded, tap_weights, length):
    running = padded[:, 0:length] * tap_weights[0]
    for tap_idx in range(1, tap_weights.shape[0]):
        running = running + padded[:, tap_idx : tap_idx + length] * tap_weights[tap_idx]
    return running


def add_rows(left_rows, running, shard_piece, offset):
    columns = lax.dynamic_slice_in_dim(left_rows, offset, shard_piece.shape[0], 1)
    return running + jnp.dot(columns, shard_piece, preferred_element_type=jnp.float32)


def project_rows(left_rows, shard_piece, offset):
    return jnp.dot(left_rows, shard_piece, preferred_element_type=jnp.float32)


def shards(
    tokens, norm_gain, val_weight, gate_weight, conv_taps, conv_bias, ln_gain, ln_shift, out_weight
):
    stream = tokens
    num_seqs = tokens.shape[0]
    local_len = tokens.shape[1]
    chan_width = val_weight.shape[2]
    all_channels = chan_width * lax.axis_size("tp")
    half_width = conv_taps.shape[1] // 2
    for layer_idx in range(LAYERS):
        gathered = lax.all_gather(stream, "tp", axis=2, tiled=True)
        widened = gathered.astype(jnp.float32)
        scaled = widened * lax.rsqrt(jnp.mean(widened * widened, axis=-1, keepdims=True) + epsilon)
        normed = (scaled * norm_gain[layer_idx]).astype(jnp.bfloat16)
        tok_rows = normed.reshape(-1, normed.shape[2])
        zeroed = jnp.zeros((tok_rows.shape[0], chan_width), jnp.float32)
        values = over_all(val_weight[layer_idx], "sp", 0, partial(add_rows, tok_rows), zeroed)
        gates = over_all(gate_weight[layer_idx], "sp", 0, partial(add_rows, tok_rows), zeroed)
        gated = (
            (values * jax.nn.sigmoid(gates))
            .astype(jnp.bfloat16)
            .reshape(num_seqs, local_len, chan_width)
        )
        padded = with_halo(gated, (("sp", 1),), half_width, False)
        convolved = (
            depthwise(padded.astype(jnp.float32), conv_taps[layer_idx], local_len)
            + conv_bias[layer_idx]
        )
        first_sum, second_sum = lax.psum(
            (jnp.sum(convolved, axis=-1), jnp.sum(convolved * convolved, axis=-1)), "tp"
        )
        mean_val = (first_sum / all_channels)[..., None]
        spread = (second_sum / all_channels)[..., None] - mean_val * mean_val
        centered = convolved - mean_val
        normalized = (
            centered * lax.rsqrt(spread + epsilon) * ln_gain[layer_idx] + ln_shift[layer_idx]
        )
        activated = jax.nn.silu(normalized).astype(jnp.bfloat16).reshape(-1, chan_width)
        partial_terms = over_all_2(out_weight[layer_idx], "sp", 1, partial(project_rows, activated))
        full_width = partial_terms.shape[1]
        summed = lax.psum_scatter(
            partial_terms.reshape(num_seqs, local_len, full_width).astype(jnp.bfloat16),
            "tp",
            scatter_dimension=2,
            tiled=True,
        ).astype(jnp.float32)
        stream = (stream.astype(jnp.float32) + summed).astype(jnp.bfloat16)
    return stream


def solution(mesh):
    placed = (
        P(None, "sp", "tp"),
        P(),
        P(None, "sp", "tp"),
        P(None, "sp", "tp"),
        P(None, None, "tp"),
        P(None, "tp"),
        P(None, "tp"),
        P(None, "tp"),
        P(None, "tp", "sp"),
    )
    return jax.shard_map(
        shards, mesh=mesh, in_specs=placed, out_specs=P(None, "sp", "tp"), check_vma=False
    )
```

profile of v0, /device:TPU:25, one launch (start us, length us, event | category | flops | bytes accessed | tf_op | source)
XLA Modules:
  0.0 498.0 jit_solution(14715837289468333107)
XLA Ops:
  6.5 0.9 fusion.211
  7.4 7.9 %all_gather.48 = bf16[4,64,1024]{2,1,0:T(8,128)(2,1)S(1)} all-gather(bf16[4,64,256]{2,1,0:T(8,128)(2,1)} %param.9), channel_id=1, replica_groups=mesh['sp'=8,'tp'=4] {'tp'}, dimensions={2}, use_global_device_ids=true | all-gather | bytes 655360 | tf_op jit(solution)/shard_map/all_gather | solution.py:62
  15.3 0.2 fusion.20
  15.5 0.7 copy-done.1
  16.3 21.8 %all-gather = bf16[1,1024,128]{2,1,0:T(8,128)(2,1)S(1)} all-gather(bf16[1,128,128]{2,1,0:T(8,128)(2,1)S(1)} %get-tuple-element.31), channel_id=2, replica_groups=mesh['sp'=8,'tp'=4] {'sp'}, dimensions={1}, use_global_device_ids=true | all-gather | bytes 294912 | tf_op jit(solution)/shard_map/all_gather | solution.py:15
  38.1 25.3 %all-gather.1 = bf16[1,1024,128]{2,1,0:T(8,128)(2,1)S(1)} all-gather(bf16[1,128,128]{2,1,0:T(8,128)(2,1)S(1)} %get-tuple-element.27), channel_id=3, replica_groups=mesh['sp'=8,'tp'=4] {'sp'}, dimensions={1}, use_global_device_ids=true | all-gather | bytes 294912 | tf_op jit(solution)/shard_map/all_gather | solution.py:15
  63.3 0.2 fusion.22
  63.5 0.3 fusion.46
  63.8 0.3 fusion.16
  64.2 5.4 %collective-permute-start = (bf16[4,15,128]{2,1,0:T(8,128)(2,1)S(1)}, bf16[4,15,128]{2,1,0:T(8,128)(2,1)S(1)}, u32[]{:S(2)}, u32[]{:S(2)}) collective-permute-start(bf16[4,15,128]{2,1,0:T(8,128)(2,1)S(1)} %get-tuple-element.43), channel_id=1, source_target_pairs={{0,4},{4,8},{8,12},{12,16},{16,20},{20,24},{24,28},{1,5},{5,9},{9,... | collective-permute-start | bytes 46088 | tf_op jit(solution)/shard_map/ppermute | solution.py:26
  69.6 1.9 collective-permute-start.1
  71.6 0.7 copy-done.5
  72.3 0.6 copy-done.6
  72.9 21.8 %all-gather.2 = bf16[1,128,1024]{2,1,0:T(8,128)(2,1)S(1)} all-gather(bf16[1,128,128]{2,1,0:T(8,128)(2,1)S(1)} %get-tuple-element.33), channel_id=4, replica_groups=mesh['sp'=8,'tp'=4] {'sp'}, dimensions={2}, use_global_device_ids=true | all-gather | bytes 294912 | tf_op jit(solution)/shard_map/all_gather | solution.py:33
  94.8 0.6 fusion.199
  95.4 24.2 %all-reduce.3 = (f32[4,64]{1,0:T(4,128)S(1)}, f32[4,64]{1,0:T(4,128)S(1)}) all-reduce(f32[4,64]{1,0:T(4,128)S(1)} %get-tuple-element.12, f32[4,64]{1,0:T(4,128)S(1)} %get-tuple-element.11), channel_id=1, replica_groups=mesh['sp'=8,'tp'=4] {'tp'}, use_global_device_ids=true, to_apply=%region_4.0 | all-reduce | flops 512 | bytes 4096 | tf_op jit(solution)/shard_map/psum | solution.py:80
  119.6 1.2 convolution_convert_fusion.3
  120.8 0.0 reduce-scatter.7.cloned.1.call-start
  120.8 25.0 %all-gather.3 = bf16[1,1024,128]{2,1,0:T(8,128)(2,1)S(1)} all-gather(bf16[1,128,128]{2,1,0:T(8,128)(2,1)S(1)} %get-tuple-element.30), channel_id=5, replica_groups=mesh['sp'=8,'tp'=4] {'sp'}, dimensions={1}, use_global_device_ids=true | all-gather | bytes 294912 | tf_op jit(solution)/shard_map/all_gather | solution.py:15
  145.9 25.4 %all-gather.4 = bf16[1,1024,128]{2,1,0:T(8,128)(2,1)S(1)} all-gather(bf16[1,128,128]{2,1,0:T(8,128)(2,1)S(1)} %get-tuple-element.26), channel_id=6, replica_groups=mesh['sp'=8,'tp'=4] {'sp'}, dimensions={1}, use_global_device_ids=true | all-gather | bytes 294912 | tf_op jit(solution)/shard_map/all_gather | solution.py:15
  171.3 0.9 add_convert_fusion.3
  172.3 18.6 %all_gather.52 = bf16[4,64,1024]{2,1,0:T(8,128)(2,1)S(1)} all-gather(bf16[4,64,256]{2,1,0:T(8,128)(2,1)S(1)} %add_convert_fusion.3), channel_id=1, replica_groups=mesh['sp'=8,'tp'=4] {'tp'}, dimensions={2}, use_global_device_ids=true | all-gather | bytes 655360 | tf_op jit(solution)/shard_map/all_gather | solution.py:62
  190.9 0.2 fusion.23
  191.1 0.2 fusion.25
  191.3 0.3 fusion.42
  191.6 0.3 fusion.17
  191.9 6.5 %collective-permute-start.2 = (bf16[4,15,128]{2,1,0:T(8,128)(2,1)S(1)}, bf16[4,15,128]{2,1,0:T(8,128)(2,1)S(1)}, u32[]{:S(2)}, u32[]{:S(2)}) collective-permute-start(bf16[4,15,128]{2,1,0:T(8,128)(2,1)S(1)} %get-tuple-element.41), channel_id=1, source_target_pairs={{0,4},{4,8},{8,12},{12,16},{16,20},{20,24},{24,28},{1,5},{5,9},{9,... | collective-permute-start | bytes 46088 | tf_op jit(solution)/shard_map/ppermute | solution.py:26
  198.4 1.9 collective-permute-start.3
  200.3 21.8 %all-gather.5 = bf16[1,128,1024]{2,1,0:T(8,128)(2,1)S(1)} all-gather(bf16[1,128,128]{2,1,0:T(8,128)(2,1)S(1)} %get-tuple-element.34), channel_id=7, replica_groups=mesh['sp'=8,'tp'=4] {'sp'}, dimensions={2}, use_global_device_ids=true | all-gather | bytes 294912 | tf_op jit(solution)/shard_map/all_gather | solution.py:33
  222.2 0.6 fusion.198
  222.8 11.8 %all-reduce.2 = (f32[4,64]{1,0:T(4,128)S(1)}, f32[4,64]{1,0:T(4,128)S(1)}) all-reduce(f32[4,64]{1,0:T(4,128)S(1)} %get-tuple-element.10, f32[4,64]{1,0:T(4,128)S(1)} %get-tuple-element.9), channel_id=1, replica_groups=mesh['sp'=8,'tp'=4] {'tp'}, use_global_device_ids=true, to_apply=%region_10.11 | all-reduce | flops 512 | bytes 4096 | tf_op jit(solution)/shard_map/psum | solution.py:80
  234.6 1.2 convolution_convert_fusion.2
  235.8 0.0 reduce-scatter.9.cloned.1.call-start
  235.8 25.0 %all-gather.6 = bf16[1,1024,128]{2,1,0:T(8,128)(2,1)S(1)} all-gather(bf16[1,128,128]{2,1,0:T(8,128)(2,1)S(1)} %get-tuple-element.32), channel_id=8, replica_groups=mesh['sp'=8,'tp'=4] {'sp'}, dimensions={1}, use_global_device_ids=true | all-gather | bytes 294912 | tf_op jit(solution)/shard_map/all_gather | solution.py:15
  260.8 25.2 %all-gather.7 = bf16[1,1024,128]{2,1,0:T(8,128)(2,1)S(1)} all-gather(bf16[1,128,128]{2,1,0:T(8,128)(2,1)S(1)} %get-tuple-element.28), channel_id=9, replica_groups=mesh['sp'=8,'tp'=4] {'sp'}, dimensions={1}, use_global_device_ids=true | all-gather | bytes 294912 | tf_op jit(solution)/shard_map/all_gather | solution.py:15
  286.1 0.9 add_convert_fusion.2
  287.0 18.6 %all_gather.56 = bf16[4,64,1024]{2,1,0:T(8,128)(2,1)S(1)} all-gather(bf16[4,64,256]{2,1,0:T(8,128)(2,1)S(1)} %add_convert_fusion.2), channel_id=1, replica_groups=mesh['sp'=8,'tp'=4] {'tp'}, dimensions={2}, use_global_device_ids=true | all-gather | bytes 655360 | tf_op jit(solution)/shard_map/all_gather | solution.py:62
  305.6 0.2 fusion.26
  305.8 0.2 fusion.28
  306.0 0.3 fusion.38
  306.3 0.3 fusion.18
  306.6 6.2 %collective-permute-start.4 = (bf16[4,15,128]{2,1,0:T(8,128)(2,1)S(1)}, bf16[4,15,128]{2,1,0:T(8,128)(2,1)S(1)}, u32[]{:S(2)}, u32[]{:S(2)}) collective-permute-start(bf16[4,15,128]{2,1,0:T(8,128)(2,1)S(1)} %get-tuple-element.39), channel_id=1, source_target_pairs={{0,4},{4,8},{8,12},{12,16},{16,20},{20,24},{24,28},{1,5},{5,9},{9,... | collective-permute-start | bytes 46088 | tf_op jit(solution)/shard_map/ppermute | solution.py:26
  312.9 1.9 collective-permute-start.5
  314.8 21.8 %all-gather.8 = bf16[1,128,1024]{2,1,0:T(8,128)(2,1)S(1)} all-gather(bf16[1,128,128]{2,1,0:T(8,128)(2,1)S(1)} %get-tuple-element.36), channel_id=10, replica_groups=mesh['sp'=8,'tp'=4] {'sp'}, dimensions={2}, use_global_device_ids=true | all-gather | bytes 294912 | tf_op jit(solution)/shard_map/all_gather | solution.py:33
  336.7 0.6 fusion.197
  337.2 11.8 %all-reduce.1 = (f32[4,64]{1,0:T(4,128)S(1)}, f32[4,64]{1,0:T(4,128)S(1)}) all-reduce(f32[4,64]{1,0:T(4,128)S(1)} %get-tuple-element.8, f32[4,64]{1,0:T(4,128)S(1)} %get-tuple-element.7), channel_id=1, replica_groups=mesh['sp'=8,'tp'=4] {'tp'}, use_global_device_ids=true, to_apply=%region_16.17 | all-reduce | flops 512 | bytes 4096 | tf_op jit(solution)/shard_map/psum | solution.py:80
  349.0 1.2 convolution_convert_fusion.1
  350.2 0.0 reduce-scatter.11.cloned.1.call-start
  350.3 25.0 %all-gather.9 = bf16[1,1024,128]{2,1,0:T(8,128)(2,1)S(1)} all-gather(bf16[1,128,128]{2,1,0:T(8,128)(2,1)S(1)} %get-tuple-element.29), channel_id=11, replica_groups=mesh['sp'=8,'tp'=4] {'sp'}, dimensions={1}, use_global_device_ids=true | all-gather | bytes 294912 | tf_op jit(solution)/shard_map/all_gather | solution.py:15
  375.3 25.2 %all-gather.10 = bf16[1,1024,128]{2,1,0:T(8,128)(2,1)S(1)} all-gather(bf16[1,128,128]{2,1,0:T(8,128)(2,1)S(1)} %get-tuple-element.25), channel_id=12, replica_groups=mesh['sp'=8,'tp'=4] {'sp'}, dimensions={1}, use_global_device_ids=true | all-gather | bytes 294912 | tf_op jit(solution)/shard_map/all_gather | solution.py:15
  400.5 0.9 add_convert_fusion.1
  401.4 18.8 %all_gather.60 = bf16[4,64,1024]{2,1,0:T(8,128)(2,1)S(1)} all-gather(bf16[4,64,256]{2,1,0:T(8,128)(2,1)S(1)} %add_convert_fusion.1), channel_id=1, replica_groups=mesh['sp'=8,'tp'=4] {'tp'}, dimensions={2}, use_global_device_ids=true | all-gather | bytes 655360 | tf_op jit(solution)/shard_map/all_gather | solution.py:62
  420.2 0.2 fusion.29
  420.4 0.2 fusion.31
  420.6 0.3 fusion.34
  420.9 0.3 fusion.19
  421.2 6.2 %collective-permute-start.6 = (bf16[4,15,128]{2,1,0:T(8,128)(2,1)S(1)}, bf16[4,15,128]{2,1,0:T(8,128)(2,1)S(1)}, u32[]{:S(2)}, u32[]{:S(2)}) collective-permute-start(bf16[4,15,128]{2,1,0:T(8,128)(2,1)S(1)} %get-tuple-element.37), channel_id=1, source_target_pairs={{0,4},{4,8},{8,12},{12,16},{16,20},{20,24},{24,28},{1,5},{5,9},{9,... | collective-permute-start | bytes 46088 | tf_op jit(solution)/shard_map/ppermute | solution.py:26
  427.5 1.9 collective-permute-start.7
  429.4 21.8 %all-gather.11 = bf16[1,128,1024]{2,1,0:T(8,128)(2,1)S(1)} all-gather(bf16[1,128,128]{2,1,0:T(8,128)(2,1)S(1)} %get-tuple-element.35), channel_id=13, replica_groups=mesh['sp'=8,'tp'=4] {'sp'}, dimensions={2}, use_global_device_ids=true | all-gather | bytes 294912 | tf_op jit(solution)/shard_map/all_gather | solution.py:33
  451.3 0.6 fusion.196
  451.8 11.8 %all-reduce = (f32[4,64]{1,0:T(4,128)S(1)}, f32[4,64]{1,0:T(4,128)S(1)}) all-reduce(f32[4,64]{1,0:T(4,128)S(1)} %get-tuple-element.6, f32[4,64]{1,0:T(4,128)S(1)} %get-tuple-element.5), channel_id=1, replica_groups=mesh['sp'=8,'tp'=4] {'tp'}, use_global_device_ids=true, to_apply=%region_22.23 | all-reduce | flops 512 | bytes 4096 | tf_op jit(solution)/shard_map/psum | solution.py:80
  463.6 1.2 convolution_convert_fusion
  464.8 25.0 %reduce-scatter.11.cloned.1.call-done = bf16[4,64,256]{2,1,0:T(8,128)(2,1)} async-done(((bf16[4,64,1024]{2,1,0:T(8,128)(2,1)}), bf16[4,64,256]{2,1,0:T(8,128)(2,1)}) %reduce-scatter.11.cloned.1.call-update) | async-done | bytes 131088 | tf_op jit(solution)/shard_map/reduce_scatter | solution.py:92
  489.9 1.6 add_convert_fusion
  (57 shorter events, 0.5 us)
Async XLA Ops:
  6.5 164.8 %reduce-scatter.5.cloned.1.call-start = ((), (), s32[]{:S(2)}) async-start(), calls=%async_computation.4 | async-start | bytes 655360 | tf_op jit(solution)/shard_map/reduce_scatter | solution.py:92
  15.3 0.9 copy-start.1
  16.2 21.8 %copy-start.2 = (bf16[4,128,128]{2,1,0:T(8,128)(2,1)S(1)}, bf16[4,128,128]{2,1,0:T(8,128)(2,1)}, u32[]{:S(2)}) copy-start(bf16[4,128,128]{2,1,0:T(8,128)(2,1)} %param.12) | copy-start | bytes 393220
  63.8 8.4 %copy-start.3 = (bf16[4,128,128]{2,1,0:T(8,128)(2,1)S(1)}, bf16[4,128,128]{2,1,0:T(8,128)(2,1)}, u32[]{:S(2)}) copy-start(bf16[4,128,128]{2,1,0:T(8,128)(2,1)} %param.17) | copy-start | bytes 393220
  64.1 7.4 %copy-start.4 = (f32[4,31,128]{2,0,1:T(4,128)S(1)}, f32[4,31,128]{2,0,1:T(4,128)}, u32[]{:S(2)}) copy-start(f32[4,31,128]{2,0,1:T(4,128)} %param.13) | copy-start | bytes 190468
  64.2 30.6 %collective-permute-start = (bf16[4,15,128]{2,1,0:T(8,128)(2,1)S(1)}, bf16[4,15,128]{2,1,0:T(8,128)(2,1)S(1)}, u32[]{:S(2)}, u32[]{:S(2)}) collective-permute-start(bf16[4,15,128]{2,1,0:T(8,128)(2,1)S(1)} %get-tuple-element.43), channel_id=1, source_target_pairs={{0,4},{4,8},{8,12},{12,16},{16,20},{20,24},{24,28},{1,5},{5,9},{9,... | collective-permute-start | bytes 46088 | tf_op jit(solution)/shard_map/ppermute | solution.py:26
  69.6 25.2 %collective-permute-start.1 = (bf16[4,15,128]{2,1,0:T(8,128)(2,1)S(1)}, bf16[4,15,128]{2,1,0:T(8,128)(2,1)S(1)}, u32[]{:S(2)}, u32[]{:S(2)}) collective-permute-start(bf16[4,15,128]{2,1,0:T(8,128)(2,1)S(1)} %get-tuple-element.44), channel_id=1, source_target_pairs={{4,0},{8,4},{12,8},{16,12},{20,16},{24,20},{28,24},{5,1},{9,5},{13... | collective-permute-start | bytes 46088 | tf_op jit(solution)/shard_map/ppermute | solution.py:27
  71.5 0.7 copy-start.5
  72.2 0.7 copy-start.6
  72.2 0.7 copy-start.7
  120.8 165.2 %reduce-scatter.7.cloned.1.call-start = ((), (), s32[]{:S(2)}) async-start(), calls=%async_computation.5 | async-start | bytes 655360 | tf_op jit(solution)/shard_map/reduce_scatter | solution.py:92
  145.9 25.5 %copy-start = (bf16[4,64,256]{2,1,0:T(8,128)(2,1)S(1)}, bf16[4,64,256]{2,1,0:T(8,128)(2,1)}, u32[]{:S(2)}) copy-start(bf16[4,64,256]{2,1,0:T(8,128)(2,1)} %param.9) | copy-start | bytes 393220
  191.9 30.2 %collective-permute-start.2 = (bf16[4,15,128]{2,1,0:T(8,128)(2,1)S(1)}, bf16[4,15,128]{2,1,0:T(8,128)(2,1)S(1)}, u32[]{:S(2)}, u32[]{:S(2)}) collective-permute-start(bf16[4,15,128]{2,1,0:T(8,128)(2,1)S(1)} %get-tuple-element.41), channel_id=1, source_target_pairs={{0,4},{4,8},{8,12},{12,16},{16,20},{20,24},{24,28},{1,5},{5,9},{9,... | collective-permute-start | bytes 46088 | tf_op jit(solution)/shard_map/ppermute | solution.py:26
  198.4 23.8 %collective-permute-start.3 = (bf16[4,15,128]{2,1,0:T(8,128)(2,1)S(1)}, bf16[4,15,128]{2,1,0:T(8,128)(2,1)S(1)}, u32[]{:S(2)}, u32[]{:S(2)}) collective-permute-start(bf16[4,15,128]{2,1,0:T(8,128)(2,1)S(1)} %get-tuple-element.42), channel_id=1, source_target_pairs={{4,0},{8,4},{12,8},{16,12},{20,16},{24,20},{28,24},{5,1},{9,5},{13... | collective-permute-start | bytes 46088 | tf_op jit(solution)/shard_map/ppermute | solution.py:27
  235.8 164.7 %reduce-scatter.9.cloned.1.call-start = ((), (), s32[]{:S(2)}) async-start(), calls=%async_computation.6 | async-start | bytes 655360 | tf_op jit(solution)/shard_map/reduce_scatter | solution.py:92
  306.6 30.0 %collective-permute-start.4 = (bf16[4,15,128]{2,1,0:T(8,128)(2,1)S(1)}, bf16[4,15,128]{2,1,0:T(8,128)(2,1)S(1)}, u32[]{:S(2)}, u32[]{:S(2)}) collective-permute-start(bf16[4,15,128]{2,1,0:T(8,128)(2,1)S(1)} %get-tuple-element.39), channel_id=1, source_target_pairs={{0,4},{4,8},{8,12},{12,16},{16,20},{20,24},{24,28},{1,5},{5,9},{9,... | collective-permute-start | bytes 46088 | tf_op jit(solution)/shard_map/ppermute | solution.py:26
  312.9 23.8 %collective-permute-start.5 = (bf16[4,15,128]{2,1,0:T(8,128)(2,1)S(1)}, bf16[4,15,128]{2,1,0:T(8,128)(2,1)S(1)}, u32[]{:S(2)}, u32[]{:S(2)}) collective-permute-start(bf16[4,15,128]{2,1,0:T(8,128)(2,1)S(1)} %get-tuple-element.40), channel_id=1, source_target_pairs={{4,0},{8,4},{12,8},{16,12},{20,16},{24,20},{28,24},{5,1},{9,5},{13... | collective-permute-start | bytes 46088 | tf_op jit(solution)/shard_map/ppermute | solution.py:27
  350.2 139.6 %reduce-scatter.11.cloned.1.call-start = ((), (), s32[]{:S(2)}) async-start(), calls=%async_computation.7 | async-start | bytes 655360 | tf_op jit(solution)/shard_map/reduce_scatter | solution.py:92
  421.2 30.0 %collective-permute-start.6 = (bf16[4,15,128]{2,1,0:T(8,128)(2,1)S(1)}, bf16[4,15,128]{2,1,0:T(8,128)(2,1)S(1)}, u32[]{:S(2)}, u32[]{:S(2)}) collective-permute-start(bf16[4,15,128]{2,1,0:T(8,128)(2,1)S(1)} %get-tuple-element.37), channel_id=1, source_target_pairs={{0,4},{4,8},{8,12},{12,16},{16,20},{20,24},{24,28},{1,5},{5,9},{9,... | collective-permute-start | bytes 46088 | tf_op jit(solution)/shard_map/ppermute | solution.py:26
  427.5 23.8 %collective-permute-start.7 = (bf16[4,15,128]{2,1,0:T(8,128)(2,1)S(1)}, bf16[4,15,128]{2,1,0:T(8,128)(2,1)S(1)}, u32[]{:S(2)}, u32[]{:S(2)}) collective-permute-start(bf16[4,15,128]{2,1,0:T(8,128)(2,1)S(1)} %get-tuple-element.38), channel_id=1, source_target_pairs={{4,0},{8,4},{12,8},{16,12},{20,16},{24,20},{28,24},{5,1},{9,5},{13... | collective-permute-start | bytes 46088 | tf_op jit(solution)/shard_map/ppermute | solution.py:27
Sparse Core Ops, SparseCore 0:
  120.9 25.0 reduce-scatter.4
  235.9 24.8 reduce-scatter.6
  350.4 25.0 reduce-scatter.8
  465.0 24.8 reduce-scatter.10
where the time goes:
time: 501 us; the launch traced here: 498 us
  blocking collectives  409 us (82%)
  starting transfers between devices  32.2 us (6%)
  waiting for transfers between devices  25.2 us (5%)
  between operations  13.5 us (3%)
  other arithmetic  8.32 us (2%)
  matrix products  7 us (1%)
    all_gather x8, blocking collectives, over_all(): lax.all_gather(a, axis, axis=dim, tiled=True)  198 us
    all_gather x4, blocking collectives, over_all_2(): return work(lax.all_gather(shard, axis, axis=dim, tiled=True), jnp.int32(0))  87.3 us
    all_gather x4, blocking collectives, shards(): gathered = lax.all_gather(stream, 'tp', axis=2, tiled=True)  63.9 us
    psum x4, blocking collectives, shards(): lax.psum((jnp.sum(convolved, axis=-1), jnp.sum(convolved * convolved, axi...  59.7 us
    reduce_scatter x4, waiting for transfers between devices, shards(): lax.psum_scatter(partial_terms.reshape(num_seqs, local_len, full_width).a...  25.1 us
    ppermute x4, starting transfers between devices, with_halo(): before = lax.ppermute(last, axis, up)  24.4 us
  transfers between devices with their start and end apart: 12, of which 1 were waited for; matrix products, arithmetic and copies ran while one was open for 0% of the time, Pallas kernels for 0%

commit v1 on v0

--- a/solution.py
+++ b/solution.py
@@ -3,7 +3,11 @@
 import jax
 import jax.numpy as jnp
 from jax import lax
+from jax.experimental import pallas as pl
+from jax.experimental.pallas import tpu as pltpu
 from jax.sharding import PartitionSpec as P
+
+MESH = pl.DeviceIdType.MESH
 
 LAYERS = 4
 
@@ -99,6 +103,339 @@
     return stream
 
 
+def stack_kernel(
+    dims, tok, gain, val_w, gate_w, taps, bias, lng, lns, out_w, out,
+    xs, vals, gates, outs, ptaps, pbias, plng, plns, gs, cv, act, stage,
+    loc_sem, tsend, trecv, psend, precv, wsend, wrecv, osend, orecv,
+):
+    SP, TP, Z, L, D, C, F, W, K, TAPS, PAD, E = dims
+    sp, tp = lax.axis_index("sp"), lax.axis_index("tp")
+    zi, yi, xi, ci = sp // 2, sp % 2, tp // 2, tp % 2
+    half = TAPS // 2
+
+    def remote(src, dst, ss, rs, to_sp, to_tp):
+        return pltpu.make_async_remote_copy(
+            src_ref=src, dst_ref=dst, send_sem=ss, recv_sem=rs,
+            device_id=(to_sp, to_tp), device_id_type=MESH,
+        )
+
+    def feat(t):
+        return pl.ds(pl.multiple_of(t * F, F), F)
+
+    finish = []
+
+    def tok_copy(side, d, to_sp):
+        to = lax.rem(tp + d, TP)
+        rows = {0: (0, L, E), 1: (L - E, E, 0), 2: (0, E, E + L)}[side]
+        return remote(
+            tok.at[to, pl.ds(rows[0], rows[1]), :],
+            xs.at[pl.ds(rows[2], rows[1]), feat(tp)],
+            tsend.at[side, d], trecv.at[side, d], to_sp, to,
+        )
+
+    own_tok = pltpu.make_async_copy(tok.at[tp], xs.at[pl.ds(E, L), feat(tp)], loc_sem.at[0])
+    own_tok.start()
+
+    @pl.when(sp == 0)
+    def _():
+        xs[pl.ds(0, E), :] = jnp.zeros((E, D), xs.dtype)
+
+    @pl.when(sp == SP - 1)
+    def _():
+        xs[pl.ds(E + L, E), :] = jnp.zeros((E, D), xs.dtype)
+
+    sources = (val_w, gate_w, out_w)
+    bufs = (vals, gates, outs)
+    units = [(l, k) for l in range(LAYERS) for k in range(3)]
+
+    def block(n, zs, ys, t):
+        l, k = units[n]
+        part = pl.ds(pl.multiple_of(t * W, W), W)
+        if k < 2:
+            return bufs[k].at[l, zs, ys, :, part]
+        return bufs[k].at[l, zs, ys, part, :]
+
+    every = slice(None)
+    sib, xpeer = xi * 2 + (1 - ci), (1 - xi) * 2 + ci
+    ypeer = zi * 2 + (1 - yi)
+
+    def y_first(n):
+        l, k = units[n]
+        return k == 0 or (k == 2 and l % 2 == 0)
+
+    own = []
+    first = []
+    for n, (l, k) in enumerate(units):
+        c = pltpu.make_async_copy(sources[k].at[l], block(n, zi, yi, tp), loc_sem.at[1 + n])
+        own.append(c)
+        first.append([
+            remote(
+                sources[k].at[l], block(n, zi, yi, tp),
+                wsend.at[n, d - 1], wrecv.at[n, d - 1], lax.rem(zi + d, Z) * 2 + yi, tp,
+            )
+            for d in range(1, Z)
+        ])
+
+    def start(n, slot, zs, ys, t, to_sp, to_tp):
+        ref = block(n, zs, ys, t)
+        c = remote(ref, ref, wsend.at[n, slot], wrecv.at[n, slot], to_sp, to_tp)
+        c.start()
+        finish.append(c)
+        return c
+
+    for c in own[:2]:
+        c.start()
+    for n in range(2):
+        for c in first[n]:
+            c.start()
+    for d in range(1, TP):
+        tok_copy(0, d, sp).start()
+    small, params = [], []
+    for i, (src, dst) in enumerate(((taps, ptaps), (bias, pbias), (lng, plng), (lns, plns))):
+        c = pltpu.make_async_copy(src, dst.at[tp], loc_sem.at[1 + len(units) + i])
+        c.start()
+        small.append(c)
+        for d in range(1, TP):
+            r = remote(src, dst.at[tp], psend.at[i, d], precv.at[i, d], sp, lax.rem(tp + d, TP))
+            r.start()
+            finish.append(r)
+            params.append(r)
+
+    @pl.when(sp < SP - 1)
+    def _():
+        for d in range(TP):
+            tok_copy(1, d, sp + 1).start()
+
+    @pl.when(sp > 0)
+    def _():
+        for d in range(TP):
+            tok_copy(2, d, sp - 1).start()
+
+    for n in range(2, len(units)):
+        own[n].start()
+        for c in first[n]:
+            c.start()
+
+    z0 = Z - 1
+    hold = {}
+
+    def step2(n):
+        own[n].wait()
+        for c in first[n]:
+            c.wait_recv()
+            finish.append(c)
+        if y_first(n):
+            hold[n] = [start(n, z0, every, yi, tp, ypeer, tp)]
+        else:
+            hold[n] = [start(n, z0, every, yi, tp, sp, xpeer)]
+        hold[n, "s"] = [start(n, z0 + 1, every, yi, tp, sp, sib)]
+
+    def step3(n):
+        for c in hold[n]:
+            c.wait_recv()
+        if y_first(n):
+            hold[n] = [start(n, z0 + 2, every, every, tp, sp, xpeer)]
+            hold[n, "s"].append(start(n, z0 + 3, every, 1 - yi, tp, sp, sib))
+        else:
+            hold[n] = [
+                start(n, z0 + 2, every, yi, tp, ypeer, tp),
+                start(n, z0 + 4, every, yi, xpeer, ypeer, tp),
+            ]
+            hold[n, "s"].append(start(n, z0 + 3, every, yi, xpeer, sp, sib))
+
+    def step4(n):
+        for c in hold[n]:
+            c.wait_recv()
+        if y_first(n):
+            hold[n, "s"].append(start(n, z0 + 5, every, every, xpeer, sp, sib))
+        else:
+            hold[n, "s"].append(start(n, z0 + 5, every, 1 - yi, tp, sp, sib))
+            hold[n, "s"].append(start(n, z0 + 6, every, 1 - yi, xpeer, sp, sib))
+
+    def step5(n):
+        for c in hold[n, "s"]:
+            c.wait_recv()
+
+    def tick(t):
+        for lag, step in enumerate((step2, step3, step4, step5)):
+            if 0 <= t - lag < len(units):
+                step(t - lag)
+
+    NC = C // 128
+
+    def gated_part(l):
+        rows, base = L + 2 * E - 2 * PAD * l, PAD * l
+        x = xs[pl.ds(base, rows), :].astype(jnp.float32)
+        scaled = x * lax.rsqrt(jnp.mean(x * x, axis=-1, keepdims=True) + epsilon)
+        normed = (scaled * gain[pl.ds(l, 1), :]).astype(jnp.bfloat16)
+        place = sp * L - E + base + lax.broadcasted_iota(jnp.int32, (rows, 256), 0)
+        inside = (place >= 0) & (place < SP * L)
+        for j in range(C // 256):
+            cols = pl.ds(j * 256, 256)
+            v = jnp.dot(normed, vals[l, :, :, :, cols].reshape(D, 256), preferred_element_type=jnp.float32)
+            g = jnp.dot(normed, gates[l, :, :, :, cols].reshape(D, 256), preferred_element_type=jnp.float32)
+            r = (v * jax.nn.sigmoid(g)).astype(jnp.bfloat16).astype(jnp.float32)
+            r = jnp.where(inside, r, 0.0)
+            gs[2 * j, pl.ds(0, rows), :] = r[:, :128]
+            gs[2 * j + 1, pl.ds(0, rows), :] = r[:, 128:]
+
+    def conv_part(l):
+        rows = L + 2 * E - 2 * PAD * (l + 1)
+
+        per = W // 128
+
+        def one(c, carry):
+            t = c // per
+            lane = pl.ds(pl.multiple_of((c % per) * 128, 128), 128) if per > 1 else slice(None)
+            acc = gs[c, pl.ds(PAD - half, rows), :] * ptaps[t, l, pl.ds(0, 1), lane]
+            for k in range(1, TAPS):
+                acc = acc + gs[c, pl.ds(PAD - half + k, rows), :] * ptaps[t, l, pl.ds(k, 1), lane]
+            cv[c, pl.ds(0, rows), :] = acc + pbias[t, pl.ds(l, 1), lane]
+            return carry
+
+        lax.fori_loop(0, NC, one, 0)
+        parts = [cv[c, pl.ds(0, rows), :] for c in range(NC)]
+        mean = jnp.sum(sum(parts[1:], parts[0]), axis=-1, keepdims=True) / C
+        cent = [p - mean for p in parts]
+        sq = [p * p for p in cent]
+        inv = lax.rsqrt(jnp.sum(sum(sq[1:], sq[0]), axis=-1, keepdims=True) / C + epsilon)
+        for c in range(NC):
+            t, lane = c // per, pl.ds((c % per) * 128, 128)
+            y = cent[c] * inv * plng[t, pl.ds(l, 1), lane] + plns[t, pl.ds(l, 1), lane]
+            act[pl.ds(0, rows), pl.ds(c * 128, 128)] = (y * jax.nn.sigmoid(y)).astype(jnp.bfloat16)
+
+    def out_part(l):
+        rows, base = L + 2 * E - 2 * PAD * (l + 1), PAD * (l + 1)
+        a = act[pl.ds(0, rows), :]
+        for z in range(Z):
+            w = jnp.concatenate([outs[l, z, 0], outs[l, z, 1]], axis=1)
+            y = jnp.dot(a, w, preferred_element_type=jnp.float32)
+            cols = pl.ds(z * 2 * K, 2 * K)
+            s = xs[pl.ds(base, rows), cols].astype(jnp.float32)
+            xs[pl.ds(base, rows), cols] = (s + y).astype(jnp.bfloat16)
+
+    for t in range(4):
+        tick(t)
+    own_tok.wait()
+    for d in range(1, TP):
+        c = tok_copy(0, d, sp)
+        c.wait_recv()
+        finish.append(c)
+    for c in small:
+        c.wait()
+    for c in params:
+        c.wait_recv()
+
+    @pl.when(sp > 0)
+    def _():
+        for d in range(TP):
+            tok_copy(1, d, sp).wait_recv()
+
+    @pl.when(sp < SP - 1)
+    def _():
+        for d in range(TP):
+            tok_copy(2, d, sp).wait_recv()
+
+    t = 4
+    for l in range(LAYERS):
+        while t <= 3 * l + 4:
+            tick(t)
+            t += 1
+        gated_part(l)
+        tick(t)
+        t += 1
+        conv_part(l)
+        out_part(l)
+
+    sends = []
+    for d in range(1, TP):
+        to = lax.rem(tp + d, TP)
+        c = remote(
+            xs.at[pl.ds(E, L), feat(to)], out.at[tp],
+            osend.at[d], orecv.at[d], sp, to,
+        )
+        c.start()
+        sends.append(c)
+    mine = pltpu.make_async_copy(xs.at[pl.ds(E, L), feat(tp)], out.at[tp], loc_sem.at[0])
+    mine.start()
+    for c in finish:
+        c.wait_send()
+
+    @pl.when(sp < SP - 1)
+    def _():
+        for d in range(TP):
+            tok_copy(1, d, sp).wait_send()
+
+    @pl.when(sp > 0)
+    def _():
+        for d in range(TP):
+            tok_copy(2, d, sp).wait_send()
+
+    mine.wait()
+    for c in sends:
+        c.wait()
+
+
+def stacked(tokens, norm_gain, val_weight, gate_weight, conv_taps, conv_bias, ln_gain, ln_shift, out_weight):
+    SP, TP = lax.axis_size("sp"), lax.axis_size("tp")
+    seqs, L, F = tokens.shape
+    D = F * TP
+    layers, K, W = val_weight.shape
+    C = W * TP
+    TAPS = conv_taps.shape[1]
+    PAD = -(-(TAPS // 2) // 16) * 16
+    E = PAD * LAYERS
+    Z = SP // 2
+    rows = L + 2 * E
+    vmem = pl.BlockSpec(memory_space=pltpu.VMEM)
+    bf16, f32 = jnp.bfloat16, jnp.float32
+    dma = pltpu.SemaphoreType.DMA
+    units = 3 * LAYERS
+    return pl.pallas_call(
+        partial(stack_kernel, (SP, TP, Z, L, D, C, F, W, K, TAPS, PAD, E)),
+        out_shape=jax.ShapeDtypeStruct(tokens.shape, tokens.dtype),
+        in_specs=[vmem] * 9,
+        out_specs=vmem,
+        scratch_shapes=[
+            pltpu.VMEM((rows, D), bf16),
+            pltpu.VMEM((LAYERS, Z, 2, K, C), bf16),
+            pltpu.VMEM((LAYERS, Z, 2, K, C), bf16),
+            pltpu.VMEM((LAYERS, Z, 2, C, K), bf16),
+            pltpu.VMEM((TP,) + conv_taps.shape, f32),
+            pltpu.VMEM((TP,) + conv_bias.shape, f32),
+            pltpu.VMEM((TP,) + conv_bias.shape, f32),
+            pltpu.VMEM((TP,) + conv_bias.shape, f32),
+            pltpu.VMEM((C // 128, rows, 128), f32),
+            pltpu.VMEM((C // 128, rows, 128), f32),
+            pltpu.VMEM((rows, C), bf16),
+            pltpu.VMEM((8, 128), f32),
+            dma((1 + units + 4,)),
+            dma((3, TP)), dma((3, TP)),
+            dma((4, TP)), dma((4, TP)),
+            dma((units, Z + 6)), dma((units, Z + 6)),
+            dma((TP,)), dma((TP,)),
+        ],
+        compiler_params=pltpu.CompilerParams(has_side_effects=True, vmem_limit_bytes=48 * 1024 * 1024),
+        name="stack",
+    )(tokens, norm_gain, val_weight, gate_weight, conv_taps, conv_bias, ln_gain, ln_shift, out_weight)
+
+
+def fits(tokens, val_weight, conv_taps):
+    SP, TP = lax.axis_size("sp"), lax.axis_size("tp")
+    seqs, L, F = tokens.shape
+    layers, K, W = val_weight.shape
+    halo = -(-(conv_taps.shape[1] // 2) // 16) * 16 * LAYERS
+    return (
+        TP == 4 and SP % 2 == 0 and seqs == TP and L >= halo and L % 16 == 0
+        and F % 128 == 0 and K % 128 == 0 and W % 128 == 0 and layers == LAYERS
+    )
+
+
+def either(tokens, norm_gain, val_weight, gate_weight, conv_taps, *rest):
+    work = stacked if fits(tokens, val_weight, conv_taps) else shards
+    return work(tokens, norm_gain, val_weight, gate_weight, conv_taps, *rest)
+
+
 def solution(mesh):
     placed = (
         P(None, "sp", "tp"),
@@ -112,5 +449,5 @@
         P(None, "tp", "sp"),
     )
     return jax.shard_map(
-        shards, mesh=mesh, in_specs=placed, out_specs=P(None, "sp", "tp"), check_vma=False
+        either, mesh=mesh, in_specs=placed, out_specs=P(None, "sp", "tp"), check_vma=False
     )

time: 501 us -> 99.9 us (0.20)
  blocking collectives: 409 us -> 0 us
  Pallas kernels: 0 us -> 94.5 us
  starting transfers between devices: 32.2 us -> 0 us
  waiting for transfers between devices: 25.2 us -> 0 us
  between operations: 13.5 us -> 0.05 us
  other arithmetic: 8.32 us -> 0 us
  matrix products: 7 us -> 0 us
    all_gather x16 -> x0, blocking collectives: 349 us -> none  [the longest x8 198 us: over_all(): lax.all_gather(a, axis, axis=dim, tiled=True)]
    pallas_call x0 -> x1, Pallas kernels: none -> 94.5 us  [stacked(): pl.pallas_call(partial(stack_kernel, (SP, TP, Z, L, D, C, F, W, K, TAPS,...]
    psum x4 -> x0, blocking collectives: 59.7 us -> none  [shards(): lax.psum((jnp.sum(convolved, axis=-1), jnp.sum(convolved * convolved, axi...]
    ppermute x8 -> x0, starting transfers between devices: 32 us -> none  [the longest x4 24.4 us: with_halo(): before = lax.ppermute(last, axis, up)]
    reduce_scatter x4 -> x0, waiting for transfers between devices: 25.1 us -> none  [shards(): lax.psum_scatter(partial_terms.reshape(num_seqs, local_len, full_width).a...]
    dot_general x12 -> x0, matrix products: 7 us -> none  [the longest x4 4.66 us: project_rows(): return jnp.dot(left_rows, shard_piece, preferred_element_type=jnp.float32)]
    convert_element_type x12 -> x0, other arithmetic: 5.27 us -> none  [the longest x4 4.41 us: shards(): stream = (stream.astype(jnp.float32) + summed).astype(jnp.bfloat16)]
  transfers between devices with their start and end apart: 12 -> 0, of which waited for: 1 -> 0; matrix products, arithmetic and copies ran while one was open for 0% -> 0% of each run, Pallas kernels for 0% -> 0%
where the time goes in v1:
time: 99.9 us; the launch traced here: 99.7 us
  Pallas kernels  94.5 us (95%)
  local copies, waits for them, and re-layouts  5.17 us (5%)
    pallas_call x1, Pallas kernels, stacked(): pl.pallas_call(partial(stack_kernel, (SP, TP, Z, L, D, C, F, W, K, TAPS,...  94.5 us
    unnamed x18, local copies, waits for them, and re-layouts  5.17 us

profile of v1, /device:TPU:25, one launch (start us, length us, event | category | flops | bytes accessed | tf_op | source)
XLA Modules:
  0.0 99.7 jit_solution(6552470633957311358)
XLA Ops:
  0.0 0.0 copy-start.7
  0.0 0.0 copy-start.6
  0.0 0.0 copy-start.5
  0.0 0.0 copy-start.4
  0.0 0.9 copy.10.taps
  0.9 0.0 copy-done.7
  0.9 0.0 copy-done.6
  0.9 0.0 copy-done.5
  0.9 0.0 copy-done.4
  0.9 0.0 copy-start
  0.9 0.9 copy-done
  1.8 0.0 copy-start.1
  1.8 0.9 copy-done.1
  2.7 0.0 copy-start.2
  2.7 0.9 copy-done.2
  3.6 0.0 copy-start.3
  3.7 0.9 copy-done.3
  4.6 94.5 %stack.1 = bf16[4,64,256]{2,1,0:T(8,128)(2,1)S(1)} custom-call(bf16[4,64,256]{2,1,0:T(8,128)(2,1)S(1)} %copy-done, f32[4,1024]{1,0:T(4,128)S(1)} %copy-done.4, bf16[4,128,128]{2,1,0:T(8,128)(2,1)S(1)} %copy-done.1, bf16[4,128,128]{2,1,0:T(8,128)(2,1)S(1)} %copy-done.2, f32[4,31,128]{2,1,0:T(8,128)S(1)} %copy.10.taps, f32[4,128]{1,0:T(4,128)S(1)} %copy-done.5, ...), custom_call_target="tpu_custom_call" | custom-call | tf_op jit(solution)/shard_map/stack/pallas_call | solution.py:394
  99.1 0.7 copy.12
Async XLA Ops:
  0.0 0.9 copy-start.7
  0.0 0.9 copy-start.6
  0.0 0.9 copy-start.5
  0.0 0.9 copy-start.4
  0.9 0.9 copy-start
  1.8 0.9 copy-start.1
  2.7 0.9 copy-start.2
  3.6 0.9 copy-start.3

commit v2 on v1

--- a/solution.py
+++ b/solution.py
@@ -10,6 +10,7 @@
 MESH = pl.DeviceIdType.MESH
 
 LAYERS = 4
+LAGS = (0, 1, 2, 3)
 
 
 epsilon = 1e-06
@@ -146,31 +147,35 @@
 
     sources = (val_w, gate_w, out_w)
     bufs = (vals, gates, outs)
-    units = [(l, k) for l in range(LAYERS) for k in range(3)]
+    units = [(l, k, h) for l in range(LAYERS) for k in range(3) for h in range(2)]
 
     def block(n, zs, ys, t):
-        l, k = units[n]
-        part = pl.ds(pl.multiple_of(t * W, W), W)
+        l, k, h = units[n]
         if k < 2:
-            return bufs[k].at[l, zs, ys, :, part]
-        return bufs[k].at[l, zs, ys, part, :]
+            return bufs[k].at[l, zs, ys, t, pl.ds(h * (K // 2), K // 2), :]
+        rows = pl.ds(pl.multiple_of(t * W + h * (W // 2), W // 2), W // 2)
+        return bufs[k].at[l, zs, ys, rows, :]
+
+    def source(n):
+        l, k, h = units[n]
+        rows = sources[k].shape[1] // 2
+        return sources[k].at[l, pl.ds(h * rows, rows), :]
 
     every = slice(None)
     sib, xpeer = xi * 2 + (1 - ci), (1 - xi) * 2 + ci
     ypeer = zi * 2 + (1 - yi)
 
     def y_first(n):
-        l, k = units[n]
-        return k == 0 or (k == 2 and l % 2 == 0)
+        return units[n][2] == 0
 
     own = []
     first = []
-    for n, (l, k) in enumerate(units):
-        c = pltpu.make_async_copy(sources[k].at[l], block(n, zi, yi, tp), loc_sem.at[1 + n])
+    for n in range(len(units)):
+        c = pltpu.make_async_copy(source(n), block(n, zi, yi, tp), loc_sem.at[1 + n])
         own.append(c)
         first.append([
             remote(
-                sources[k].at[l], block(n, zi, yi, tp),
+                source(n), block(n, zi, yi, tp),
                 wsend.at[n, d - 1], wrecv.at[n, d - 1], lax.rem(zi + d, Z) * 2 + yi, tp,
             )
             for d in range(1, Z)
@@ -183,9 +188,9 @@
         finish.append(c)
         return c
 
-    for c in own[:2]:
+    for c in own[:4]:
         c.start()
-    for n in range(2):
+    for n in range(4):
         for c in first[n]:
             c.start()
     for d in range(1, TP):
@@ -211,7 +216,7 @@
         for d in range(TP):
             tok_copy(2, d, sp - 1).start()
 
-    for n in range(2, len(units)):
+    for n in range(4, len(units)):
         own[n].start()
         for c in first[n]:
             c.start()
@@ -257,9 +262,10 @@
             c.wait_recv()
 
     def tick(t):
-        for lag, step in enumerate((step2, step3, step4, step5)):
-            if 0 <= t - lag < len(units):
-                step(t - lag)
+        for lag, step in zip(LAGS, (step2, step3, step4, step5)):
+            for h in range(2):
+                if 0 <= t - lag < len(units) // 2:
+                    step(2 * (t - lag) + h)
 
     NC = C // 128
 
@@ -271,9 +277,12 @@
         place = sp * L - E + base + lax.broadcasted_iota(jnp.int32, (rows, 256), 0)
         inside = (place >= 0) & (place < SP * L)
         for j in range(C // 256):
-            cols = pl.ds(j * 256, 256)
-            v = jnp.dot(normed, vals[l, :, :, :, cols].reshape(D, 256), preferred_element_type=jnp.float32)
-            g = jnp.dot(normed, gates[l, :, :, :, cols].reshape(D, 256), preferred_element_type=jnp.float32)
+            vw, gw = (
+                jnp.concatenate([b[l, :, :, 2 * j + i].reshape(D, W) for i in range(2)], axis=1)
+                for b in (vals, gates)
+            )
+            v = jnp.dot(normed, vw, preferred_element_type=jnp.float32)
+            g = jnp.dot(normed, gw, preferred_element_type=jnp.float32)
             r = (v * jax.nn.sigmoid(g)).astype(jnp.bfloat16).astype(jnp.float32)
             r = jnp.where(inside, r, 0.0)
             gs[2 * j, pl.ds(0, rows), :] = r[:, :128]
@@ -314,37 +323,41 @@
             s = xs[pl.ds(base, rows), cols].astype(jnp.float32)
             xs[pl.ds(base, rows), cols] = (s + y).astype(jnp.bfloat16)
 
-    for t in range(4):
-        tick(t)
-    own_tok.wait()
-    for d in range(1, TP):
-        c = tok_copy(0, d, sp)
-        c.wait_recv()
-        finish.append(c)
-    for c in small:
-        c.wait()
-    for c in params:
-        c.wait_recv()
-
-    @pl.when(sp > 0)
-    def _():
-        for d in range(TP):
-            tok_copy(1, d, sp).wait_recv()
-
-    @pl.when(sp < SP - 1)
-    def _():
-        for d in range(TP):
-            tok_copy(2, d, sp).wait_recv()
-
-    t = 4
+    def arrived():
+        own_tok.wait()
+        for d in range(1, TP):
+            c = tok_copy(0, d, sp)
+            c.wait_recv()
+            finish.append(c)
+        for c in small:
+            c.wait()
+        for c in params:
+            c.wait_recv()
+
+        @pl.when(sp > 0)
+        def _():
+            for d in range(TP):
+                tok_copy(1, d, sp).wait_recv()
+
+        @pl.when(sp < SP - 1)
+        def _():
+            for d in range(TP):
+                tok_copy(2, d, sp).wait_recv()
+
+    t, last = 0, LAGS[-1]
     for l in range(LAYERS):
-        while t <= 3 * l + 4:
+        while t <= 3 * l + 1 + last:
             tick(t)
             t += 1
+        if l == 0:
+            arrived()
         gated_part(l)
         tick(t)
         t += 1
         conv_part(l)
+        if l + 1 < LAYERS:
+            tick(t)
+            t += 1
         out_part(l)
 
     sends = []
@@ -390,7 +403,7 @@
     vmem = pl.BlockSpec(memory_space=pltpu.VMEM)
     bf16, f32 = jnp.bfloat16, jnp.float32
     dma = pltpu.SemaphoreType.DMA
-    units = 3 * LAYERS
+    units = 6 * LAYERS
     return pl.pallas_call(
         partial(stack_kernel, (SP, TP, Z, L, D, C, F, W, K, TAPS, PAD, E)),
         out_shape=jax.ShapeDtypeStruct(tokens.shape, tokens.dtype),
@@ -398,8 +411,8 @@
         out_specs=vmem,
         scratch_shapes=[
             pltpu.VMEM((rows, D), bf16),
-            pltpu.VMEM((LAYERS, Z, 2, K, C), bf16),
-            pltpu.VMEM((LAYERS, Z, 2, K, C), bf16),
+            pltpu.VMEM((LAYERS, Z, 2, TP, K, W), bf16),
+            pltpu.VMEM((LAYERS, Z, 2, TP, K, W), bf16),
             pltpu.VMEM((LAYERS, Z, 2, C, K), bf16),
             pltpu.VMEM((TP,) + conv_taps.shape, f32),
             pltpu.VMEM((TP,) + conv_bias.shape, f32),
@@ -427,7 +440,7 @@
     halo = -(-(conv_taps.shape[1] // 2) // 16) * 16 * LAYERS
     return (
         TP == 4 and SP % 2 == 0 and seqs == TP and L >= halo and L % 16 == 0
-        and F % 128 == 0 and K % 128 == 0 and W % 128 == 0 and layers == LAYERS
+        and F % 128 == 0 and K % 128 == 0 and W == 128 and layers == LAYERS
     )
 
 

time: 99.9 us -> 86.7 us (0.87)
  Pallas kernels: 94.5 us -> 80.6 us
    pallas_call x1, Pallas kernels: 94.5 us -> 80.6 us  [stacked(): pl.pallas_call(partial(stack_kernel, (SP, TP, Z, L, D, C, F, W, K, TAPS,...]
where the time goes in v2:
time: 86.7 us; the launch traced here: 85.8 us
  Pallas kernels  80.6 us (93%)
  local copies, waits for them, and re-layouts  5.17 us (6%)
    pallas_call x1, Pallas kernels, stacked(): pl.pallas_call(partial(stack_kernel, (SP, TP, Z, L, D, C, F, W, K, TAPS,...  80.6 us
    unnamed x18, local copies, waits for them, and re-layouts  5.17 us

profile of v2, /device:TPU:25, one launch (start us, length us, event | category | flops | bytes accessed | tf_op | source)
XLA Modules:
  0.0 85.8 jit_solution(122955561976757568)
XLA Ops:
  0.0 0.0 copy-start.7
  0.0 0.0 copy-start.6
  0.0 0.0 copy-start.5
  0.0 0.0 copy-start.4
  0.0 0.9 %copy.10.taps = f32[4,31,128]{2,1,0:T(8,128)S(1)} copy(f32[4,31,128]{2,0,1:T(4,128)} %param.13) | data formatting | bytes 126976 | tf_op args[4]
  0.9 0.0 copy-done.7
  0.9 0.0 copy-done.6
  0.9 0.0 copy-done.5
  0.9 0.0 copy-done.4
  0.9 0.0 copy-start
  0.9 0.9 %copy-done = bf16[4,64,256]{2,1,0:T(8,128)(2,1)S(1)} copy-done((bf16[4,64,256]{2,1,0:T(8,128)(2,1)S(1)}, bf16[4,64,256]{2,1,0:T(8,128)(2,1)}, u32[]{:S(2)}) %copy-start) | copy-done | bytes 131096
  1.8 0.0 copy-start.1
  1.8 0.9 %copy-done.1 = bf16[4,128,128]{2,1,0:T(8,128)(2,1)S(1)} copy-done((bf16[4,128,128]{2,1,0:T(8,128)(2,1)S(1)}, bf16[4,128,128]{2,1,0:T(8,128)(2,1)}, u32[]{:S(2)}) %copy-start.1) | copy-done | bytes 131096
  2.7 0.0 copy-start.2
  2.7 0.9 %copy-done.2 = bf16[4,128,128]{2,1,0:T(8,128)(2,1)S(1)} copy-done((bf16[4,128,128]{2,1,0:T(8,128)(2,1)S(1)}, bf16[4,128,128]{2,1,0:T(8,128)(2,1)}, u32[]{:S(2)}) %copy-start.2) | copy-done | bytes 131096
  3.6 0.0 copy-start.3
  3.7 0.9 %copy-done.3 = bf16[4,128,128]{2,1,0:T(8,128)(2,1)S(1)} copy-done((bf16[4,128,128]{2,1,0:T(8,128)(2,1)S(1)}, bf16[4,128,128]{2,1,0:T(8,128)(2,1)}, u32[]{:S(2)}) %copy-start.3) | copy-done | bytes 131096
  4.6 80.6 %stack.1 = bf16[4,64,256]{2,1,0:T(8,128)(2,1)S(1)} custom-call(bf16[4,64,256]{2,1,0:T(8,128)(2,1)S(1)} %copy-done, f32[4,1024]{1,0:T(4,128)S(1)} %copy-done.4, bf16[4,128,128]{2,1,0:T(8,128)(2,1)S(1)} %copy-done.1, bf16[4,128,128]{2,1,0:T(8,128)(2,1)S(1)} %copy-done.2, f32[4,31,128]{2,1,0:T(8,128)S(1)} %copy.10.taps, f32[4,128]{1,0:T(4,128)S(1)} %copy-done.5, ...), custom_call_target="tpu_custom_call" | custom-call | tf_op jit(solution)/shard_map/stack/pallas_call | solution.py:407
  85.2 0.7 copy.12
Async XLA Ops:
  0.0 0.9 %copy-start.7 = (f32[4,128]{1,0:T(4,128)S(1)}, f32[4,128]{1,0:T(4,128)}, u32[]{:S(2)}) copy-start(f32[4,128]{1,0:T(4,128)} %lns.1) | copy-start | bytes 6148
  0.0 0.9 %copy-start.6 = (f32[4,128]{1,0:T(4,128)S(1)}, f32[4,128]{1,0:T(4,128)}, u32[]{:S(2)}) copy-start(f32[4,128]{1,0:T(4,128)} %lng.1) | copy-start | bytes 6148
  0.0 0.9 %copy-start.5 = (f32[4,128]{1,0:T(4,128)S(1)}, f32[4,128]{1,0:T(4,128)}, u32[]{:S(2)}) copy-start(f32[4,128]{1,0:T(4,128)} %bias.1) | copy-start | bytes 6148
  0.0 0.9 %copy-start.4 = (f32[4,1024]{1,0:T(4,128)S(1)}, f32[4,1024]{1,0:T(4,128)}, u32[]{:S(2)}) copy-start(f32[4,1024]{1,0:T(4,128)} %gain.1) | copy-start | bytes 49156
  0.9 0.9 %copy-start = (bf16[4,64,256]{2,1,0:T(8,128)(2,1)S(1)}, bf16[4,64,256]{2,1,0:T(8,128)(2,1)}, u32[]{:S(2)}) copy-start(bf16[4,64,256]{2,1,0:T(8,128)(2,1)} %tok.1) | copy-start | bytes 393220
  1.8 0.9 %copy-start.1 = (bf16[4,128,128]{2,1,0:T(8,128)(2,1)S(1)}, bf16[4,128,128]{2,1,0:T(8,128)(2,1)}, u32[]{:S(2)}) copy-start(bf16[4,128,128]{2,1,0:T(8,128)(2,1)} %val_w.1) | copy-start | bytes 393220
  2.7 0.9 %copy-start.2 = (bf16[4,128,128]{2,1,0:T(8,128)(2,1)S(1)}, bf16[4,128,128]{2,1,0:T(8,128)(2,1)}, u32[]{:S(2)}) copy-start(bf16[4,128,128]{2,1,0:T(8,128)(2,1)} %gate_w.1) | copy-start | bytes 393220
  3.6 0.9 %copy-start.3 = (bf16[4,128,128]{2,1,0:T(8,128)(2,1)S(1)}, bf16[4,128,128]{2,1,0:T(8,128)(2,1)}, u32[]{:S(2)}) copy-start(bf16[4,128,128]{2,1,0:T(8,128)(2,1)} %out_w.1) | copy-start | bytes 393220
